TPU v7x, 32 devices: a whole 2x2x4 slice. The times are simulated.
32 devices in a mesh: grp: 2 (over y), fs: 8 (over z, core), tp: 2 (over x).
Axes of the slice: x: 2, y: 2, z: 4, core: 2. Of those that a mesh axis runs over, the one named last changes fastest.
Arguments:
- tokens: bfloat16 [3584, 2048], P(('grp', 'fs'), 'tp'), parts along dimension 0, may hold values from -170 to 170
- routes: int32 [3584, 6], P(('grp', 'fs')), parts along dimension 0, may hold values from 0 to 15, all different within a row; in each aligned block of 224 rows (0 to 223, 224 to 447, ...) at most 112 rows name the same one
- route_weights: float32 [3584, 6], P(('grp', 'fs')), parts along dimension 0, may hold values from 0.2 to 1
- norm_gain: float32 [2048], P('fs'), may hold values from 0.1 to 1.9
- gate_experts: float32 [16, 2048, 512], P(None, 'fs', 'tp'), may hold values from -0.125 to 0.125
- up_experts: float32 [16, 2048, 512], P(None, 'fs', 'tp'), may hold values from -0.125 to 0.125
- down_experts: float32 [16, 512, 2048], P(None, 'fs', 'tp'), may hold values from -0.25 to 0.25
- shared_gate: float32 [2048, 512], P('fs', 'tp'), may hold values from -0.125 to 0.125
- shared_up: float32 [2048, 512], P('fs', 'tp'), may hold values from -0.125 to 0.125
- shared_down: float32 [512, 2048], P('fs', 'tp'), may hold values from -0.25 to 0.25
Outputs:
- mixed: bfloat16 [3584, 2048], P(('grp', 'fs'), 'tp'), parts along dimension 0
- gate_ready: bfloat16 [32, 2048, 512], P(('grp', 'fs'), None, 'tp'), parts along dimension 0
- up_ready: bfloat16 [32, 2048, 512], P(('grp', 'fs'), None, 'tp'), parts along dimension 0
- down_ready: bfloat16 [32, 512, 2048], P(('grp', 'fs'), 'tp'), parts along dimension 0
- shared_gate_ready: bfloat16 [4096, 512], P('grp', 'tp'), parts along dimension 0
- shared_up_ready: bfloat16 [4096, 512], P('grp', 'tp'), parts along dimension 0
- shared_down_ready: bfloat16 [1024, 2048], P(('grp', 'tp')), parts along dimension 0
There are 2 independent parts, one for each index of `grp`. A program takes and returns all parts, laid end to end along the dimension named above; an argument that names none is the same for every part. Nothing has to cross between parts.
Inputs may be any that keep to these rules, and one draw needn't show every extreme that they name: `routes`: the 6 experts of a row differ; among the rows of one index of fs no expert is named more than 112 times, a bound that some block reaches.
All inputs are finite; a program needn't handle non-finite values.
Results may differ from a plain program's by a relative error of at most 0.013.
Values may be sent and summed in bfloat16 or wider, within the bound.
A program may use at most 128 MiB of HBM per device.

v0:
```python
import jax
import jax.numpy as jnp
from jax import lax
from jax.sharding import PartitionSpec as P


def per_device(
    tokens,
    routes,
    route_weights,
    norm_gain,
    gate_experts,
    up_experts,
    down_experts,
    shared_gate,
    shared_up,
    shared_down,
):
    gain_rows = norm_gain[None, :, None]
    gate_cast = (gate_experts * gain_rows).astype(jnp.bfloat16)
    up_cast = (up_experts * gain_rows).astype(jnp.bfloat16)
    down_cast = down_experts.astype(jnp.bfloat16)
    gate_local, up_local = (
        lax.all_to_all(gate_cast, "fs", split_axis=0, concat_axis=1, tiled=True),
        lax.all_to_all(up_cast, "fs", split_axis=0, concat_axis=1, tiled=True),
    )
    down_local = lax.all_to_all(
        lax.all_to_all(down_cast, "fs", split_axis=0, concat_axis=1, tiled=True),
        "tp",
        split_axis=1,
        concat_axis=2,
        tiled=True,
    )
    shared_gate_cast = (shared_gate * norm_gain[:, None]).astype(jnp.bfloat16)
    shared_up_cast = (shared_up * norm_gain[:, None]).astype(jnp.bfloat16)
    shared_down_cast = shared_down.astype(jnp.bfloat16)
    shared_gate_local, shared_up_local, shared_down_rows = (
        lax.all_gather(shared_gate_cast, "fs", axis=0, tiled=True),
        lax.all_gather(shared_up_cast, "fs", axis=0, tiled=True),
        lax.all_gather(shared_down_cast, "fs", axis=0, tiled=True),
    )
    shared_down_local = lax.all_to_all(
        shared_down_rows, "tp", split_axis=0, concat_axis=1, tiled=True
    )
    gathered = lax.all_gather(tokens, "tp", axis=1, tiled=True)
    widened = gathered.astype(jnp.float32)
    normed = (
        widened * lax.rsqrt(jnp.mean(widened * widened, axis=1, keepdims=True) + 1e-06)
    ).astype(jnp.bfloat16)
    shared_active = (
        jax.nn.silu(jnp.dot(normed, shared_gate_local, preferred_element_type=jnp.float32))
        * jnp.dot(normed, shared_up_local, preferred_element_type=jnp.float32)
    ).astype(jnp.bfloat16)
    shared_rows = lax.psum_scatter(
        jnp.dot(shared_active, shared_down_local, preferred_element_type=jnp.float32).astype(
            jnp.bfloat16
        ),
        "tp",
        scatter_dimension=1,
        tiled=True,
    ).astype(jnp.float32)
    tok_rows, top_count = routes.shape
    experts_all = gate_experts.shape[0]
    capacity = 4 * tok_rows * top_count // (3 * experts_all)
    fs_count = lax.axis_size("fs")
    held = experts_all // fs_count
    quarter = tokens.shape[1]
    flat_routes = routes.reshape(-1)
    onehot = (flat_routes[:, None] == jnp.arange(experts_all, dtype=jnp.int32)[None, :]).astype(
        jnp.int32
    )
    earlier = jnp.cumsum(onehot, axis=0) - onehot
    slot_index = jnp.sum(earlier * onehot, axis=1)
    target = flat_routes * capacity + slot_index
    source = (
        jnp.full((experts_all * capacity,), -1, jnp.int32)
        .at[target]
        .set(jnp.arange(tok_rows * top_count, dtype=jnp.int32) // top_count)
    )
    present = (source >= 0)[:, None]
    safe_source = jnp.maximum(source, 0)
    own_part = lax.dynamic_slice_in_dim(normed, lax.axis_index("tp") * quarter, quarter, 1)
    send_rows = jnp.where(present, own_part[safe_source], jnp.zeros((), jnp.bfloat16))
    send_rows = send_rows.reshape(fs_count, held, capacity, quarter)
    received = lax.all_to_all(send_rows, "fs", split_axis=0, concat_axis=0, tiled=True)
    received = lax.all_gather(received, "tp", axis=3, tiled=True)
    gate_hidden = jnp.einsum(
        "sjcd,jdf->sjcf", received, gate_local, preferred_element_type=jnp.float32
    )
    up_hidden = jnp.einsum("sjcd,jdf->sjcf", received, up_local, preferred_element_type=jnp.float32)
    active = (jax.nn.silu(gate_hidden) * up_hidden).astype(jnp.bfloat16)
    partial_rows = jnp.einsum(
        "sjcf,jfd->sjcd", active, down_local, preferred_element_type=jnp.float32
    )
    summed = lax.psum_scatter(
        partial_rows.astype(jnp.bfloat16), "tp", scatter_dimension=3, tiled=True
    )
    returned = lax.all_to_all(summed, "fs", split_axis=0, concat_axis=0, tiled=True)
    picked = returned.reshape(experts_all * capacity, quarter)[target].reshape(
        tok_rows, top_count, quarter
    )
    weighted = jnp.einsum("tkd,tk->td", picked.astype(jnp.float32), route_weights)
    mixed = (weighted + shared_rows).astype(jnp.bfloat16)
    return (
        mixed,
        gate_local,
        up_local,
        down_local,
        shared_gate_local,
        shared_up_local,
        shared_down_local,
    )


def solution(mesh):
    return jax.shard_map(
        per_device,
        mesh=mesh,
        in_specs=(
            P(("grp", "fs"), "tp"),
            P(("grp", "fs"), None),
            P(("grp", "fs"), None),
            P("fs"),
            P(None, "fs", "tp"),
            P(None, "fs", "tp"),
            P(None, "fs", "tp"),
            P("fs", "tp"),
            P("fs", "tp"),
            P("fs", "tp"),
        ),
        out_specs=(
            P(("grp", "fs"), "tp"),
            P(("grp", "fs"), None, "tp"),
            P(("grp", "fs"), None, "tp"),
            P(("grp", "fs"), "tp", None),
            P("grp", "tp"),
            P("grp", "tp"),
            P(("grp", "tp"), None),
        ),
        check_vma=False,
    )
```

profile of v0, /device:TPU:0, one launch (start us, length us, event | category | flops | bytes accessed | tf_op | source)
XLA Modules:
  0.0 555.1 jit_solution(2266715627463554693)
XLA Ops:
  7.2 6.5 %multiply_convert_fusion = (bf16[16,256,256]{2,1,0:T(8,128)(2,1)}, bf16[16,256,256]{2,1,0:T(8,128)(2,1)}) fusion(f32[16,256,256]{2,1,0:T(8,128)} %param.15, f32[256]{0:T(256)} %param.13, f32[16,256,256]{2,1,0:T(8,128)} %param.14), kind=kLoop, calls=%fused_computation.4 | loop fusion | flops 4194304 | bytes 12583936 | tf_op jit(solution)/shard_map/convert_element_type | solution.py:21
  13.7 6.5 %all-to-all-start = ((bf16[16,256,256]{2,1,0:T(8,128)(2,1)}), bf16[16,256,256]{2,1,0:T(8,128)(2,1)S(1)}, u32[]{:S(2)}, u32[]{:S(2)}) async-start(bf16[16,256,256]{2,1,0:T(8,128)(2,1)} %get-tuple-element.17), calls=%async_computation | async-start | bytes 4194304 | tf_op jit(solution)/shard_map/all_to_all | solution.py:24
  20.2 0.1 copy.51
  20.3 0.1 eq.22
  20.5 4.5 reduce-window.6
  25.1 0.4 slice_reduce_fusion
  25.5 0.2 reduce-window.9
  25.7 0.1 broadcast_add_fusion
  25.9 0.1 copy.50
  26.0 0.1 mul.79
  26.2 7.6 %scatter_custom_fusion = s32[1792]{0:T(1024)S(1)} fusion(s32[1344]{0:T(1024)S(1)} %fusion.21, s32[1344]{0:T(1024)S(1)} %add_select_fusion, s32[]{:T(128)} %constant.15.clone.1), kind=kCustom, calls=%fused_computation.56 | custom fusion | bytes 7172 | tf_op jit(solution)/shard_map/scatter | solution.py:78
  33.9 0.1 broadcast_in_dim.29
  34.0 13.6 %all_gather.15 = bf16[224,2048]{1,0:T(8,128)(2,1)S(1)} all-gather(bf16[224,1024]{1,0:T(8,128)(2,1)S(1)} %copy-done.2), channel_id=1, replica_groups=mesh['grp'=2,'fs'=8,'tp'=2] {'tp'}, dimensions={1}, use_global_device_ids=true | all-gather | bytes 1376256 | tf_op jit(solution)/shard_map/all_gather | solution.py:45
  47.6 0.3 fusion.1
  47.9 0.2 fusion.2
  48.1 6.6 %gather_fusion = bf16[1792,1024]{1,0:T(8,128)(2,1)} fusion(bf16[224,1024]{1,0:T(8,128)(2,1)S(1)} %constant_dynamic-slice_fusion, s32[2048]{0:T(1024)S(1)} %pad_clamp_fusion.1), kind=kCustom, calls=%fused_computation | custom fusion | bytes 7347200 | tf_op jit(solution)/shard_map/gather | solution.py:83
  54.8 3.5 broadcast_select_fusion
  58.3 10.9 %all-to-all-done = bf16[16,256,256]{2,1,0:T(8,128)(2,1)S(1)} async-done(((bf16[16,256,256]{2,1,0:T(8,128)(2,1)}), bf16[16,256,256]{2,1,0:T(8,128)(2,1)S(1)}, u32[]{:S(2)}, u32[]{:S(2)}) %all-to-all-start) | async-done | bytes 2097184 | tf_op jit(solution)/shard_map/all_to_all | solution.py:24
  69.2 4.5 all-to-all-start.1
  73.7 3.8 convert_element_type.56
  77.6 78.9 %all-to-all-done.1 = bf16[8,2,112,1024]{3,2,1,0:T(8,128)(2,1)} async-done(((bf16[8,2,112,1024]{3,2,1,0:T(8,128)(2,1)}), bf16[8,2,112,1024]{3,2,1,0:T(8,128)(2,1)}, u32[]{:S(2)}, u32[]{:S(2)}) %all-to-all-start.1) | async-done | bytes 3670048 | tf_op jit(solution)/shard_map/all_to_all | solution.py:85
  156.5 4.3 all-to-all-start.3
  160.9 4.4 copy.52
  165.4 44.5 %all-to-all-done.3 = bf16[16,64,1024]{2,1,0:T(8,128)(2,1)} async-done(((bf16[16,64,1024]{2,1,0:T(8,128)(2,1)}), bf16[16,64,1024]{2,1,0:T(8,128)(2,1)}, u32[]{:S(2)}, u32[]{:S(2)}) %all-to-all-start.3) | async-done | bytes 2097184 | tf_op jit(solution)/shard_map/all_to_all | solution.py:28
  209.9 4.4 all-to-all-start.2
  214.2 1.8 copy.54
  216.0 3.5 copy.55
  219.5 43.8 %all-to-all-done.2 = bf16[16,256,256]{2,1,0:T(8,128)(2,1)} async-done(((bf16[16,256,256]{2,1,0:T(8,128)(2,1)}), bf16[16,256,256]{2,1,0:T(8,128)(2,1)}, u32[]{:S(2)}, u32[]{:S(2)}) %all-to-all-start.2) | async-done | bytes 2097184 | tf_op jit(solution)/shard_map/all_to_all | solution.py:25
  263.3 4.8 all-to-all-start.4
  268.1 0.0 all-gather.11.cloned.1.call-start
  268.2 0.7 convert_element_type.62
  268.9 0.2 reduce-scatter.3.cloned.1.call-start
  269.1 1.5 copy.49
  270.5 3.1 copy.53
  273.6 19.4 %all-to-all-done.4 = bf16[2,512,1024]{2,0,1:T(2,128)(2,1)} async-done(((bf16[2,512,1024]{2,0,1:T(2,128)(2,1)}), bf16[2,512,1024]{2,0,1:T(2,128)(2,1)}, u32[]{:S(2)}, u32[]{:S(2)}) %all-to-all-start.4) | async-done | bytes 2097184 | tf_op jit(solution)/shard_map/all_to_all | solution.py:27
  293.0 2.2 copy.56
  295.2 3.5 copy.57
  298.7 4.5 reshape.114
  303.2 7.0 %fusion.26 = f32[2,256,8,112]{1,3,2,0:T(8,128)} fusion(bf16[2,2048,256,1]{2,1,3,0:T(8,128)(2,1)} %bitcast.88, bf16[8,2,112,2048]{3,2,0,1:T(8,128)(2,1)} %all-gather.5.cloned.1.call-done), kind=kOutput, calls=%fused_computation.62 | convolution fusion | flops 1879048192 | bytes 11272192 | tf_op jit(solution)/shard_map/sjcd,jdf->sjcf/dot_general | solution.py:87
  310.2 11.9 %convert_bitcast_fusion = bf16[8,2,112,2048]{3,2,0,1:T(8,128)(2,1)} fusion(bf16[2,256,2048,1]{2,1,0,3:T(8,128)(2,1)} %reshape.114, f32[2,256,8,112]{1,3,2,0:T(8,128)} %fusion.26, bf16[2,2048,256,1]{2,1,3,0:T(8,128)(2,1)} %bitcast.90, bf16[8,2,112,2048]{3,2,0,1:T(8,128)(2,1)} %all-gather.5.cloned.1.call-done), kind=kOutput, calls=%fused_computation.3 | convolution fusion | flops 3764518912 | bytes 20709376 | tf_op jit(solution)/shard_map/sjcf,jfd->sjcd/dot_general | solution.py:92
  322.2 4.4 all-to-all-start.6
  326.6 93.3 %reduce-scatter.3.cloned.1.call-done = bf16[8,2,112,1024]{3,2,0,1:T(8,128)(2,1)} async-done(((bf16[8,2,112,2048]{3,2,0,1:T(8,128)(2,1)}), bf16[8,2,112,1024]{3,2,0,1:T(8,128)(2,1)}) %reduce-scatter.3.cloned.1.call-update) | async-done | bytes 3670032 | tf_op jit(solution)/shard_map/reduce_scatter | solution.py:95
  419.9 4.3 copy.58
  424.2 4.6 all-to-all-start.5
  428.9 0.0 all-gather.7.cloned.1.call-start
  429.0 1.8 multiply_convert_fusion.3
  430.7 0.0 all-gather.9.cloned.1.call-start
  430.8 0.5 all-gather.9.cloned.1.call-update
  431.3 0.3 reduce-scatter.5.cloned.1.call-start
  431.6 32.6 %all-gather.7.cloned.1.call-done = bf16[2048,256]{1,0:T(8,128)(2,1)} async-done(((bf16[256,256]{1,0:T(8,128)(2,1)}), bf16[2048,256]{1,0:T(8,128)(2,1)}) %all-gather.7.cloned.1.call-update) | async-done | bytes 1048592 | tf_op jit(solution)/shard_map/all_gather | solution.py:38
  464.2 1.6 fusion.28
  465.8 2.3 copy.59
  468.1 47.4 %all-gather.9.cloned.1.call-done = bf16[2048,256]{1,0:T(8,128)(2,1)} async-done(((bf16[256,256]{1,0:T(8,128)(2,1)}), bf16[2048,256]{1,0:T(8,128)(2,1)}) %all-gather.9.cloned.1.call-update) | async-done | bytes 1048592 | tf_op jit(solution)/shard_map/all_gather | solution.py:39
  515.4 3.7 convolution_convert_fusion
  519.1 0.2 copy.64
  519.3 2.3 copy.60
  521.6 1.6 copy.66
  523.1 5.3 all-to-all-done.5
  528.5 9.8 %gather_fusion.1 = bf16[1344,1024]{1,0:T(8,128)(2,1)S(1)} fusion(bf16[1792,1024]{1,0:T(8,128)(2,1)} %bitcast.21, s32[2048]{0:T(1024)S(1)} %pad_clamp_fusion), kind=kCustom, calls=%fused_computation.1 | custom fusion | bytes 5510400 | tf_op jit(solution)/shard_map/gather | solution.py:99
  538.3 2.7 reshape.85
  541.0 3.2 fusion.27
  544.2 2.1 fusion.8
  546.4 1.0 copy.73
  547.3 1.0 copy.74
  (40 shorter events, 0.4 us)
Async XLA Ops:
  13.7 6.5 %copy-start.5 = (s32[224,6]{0,1:T(8,128)S(1)}, s32[224,6]{0,1:T(8,128)}, u32[]{:S(2)}) copy-start(s32[224,6]{0,1:T(8,128)} %param.11) | copy-start | bytes 16132
  13.7 20.3 %copy-start.2 = (bf16[224,1024]{1,0:T(8,128)(2,1)S(1)}, bf16[224,1024]{1,0:T(8,128)(2,1)}, u32[]{:S(2)}) copy-start(bf16[224,1024]{1,0:T(8,128)(2,1)} %param.10) | copy-start | bytes 1376260
  13.7 55.5 %all-to-all-start = ((bf16[16,256,256]{2,1,0:T(8,128)(2,1)}), bf16[16,256,256]{2,1,0:T(8,128)(2,1)S(1)}, u32[]{:S(2)}, u32[]{:S(2)}) async-start(bf16[16,256,256]{2,1,0:T(8,128)(2,1)} %get-tuple-element.17), calls=%async_computation | async-start | bytes 4194304 | tf_op jit(solution)/shard_map/all_to_all | solution.py:24
  69.2 87.3 %all-to-all-start.1 = ((bf16[8,2,112,1024]{3,2,1,0:T(8,128)(2,1)}), bf16[8,2,112,1024]{3,2,1,0:T(8,128)(2,1)}, u32[]{:S(2)}, u32[]{:S(2)}) async-start(bf16[8,2,112,1024]{3,2,1,0:T(8,128)(2,1)} %broadcast_select_fusion), calls=%async_computation.1 | async-start | bytes 7340032 | tf_op jit(solution)/shard_map/all_to_all | solution.py:85
  156.5 53.4 %all-to-all-start.3 = ((bf16[16,64,1024]{2,1,0:T(8,128)(2,1)}), bf16[16,64,1024]{2,1,0:T(8,128)(2,1)}, u32[]{:S(2)}, u32[]{:S(2)}) async-start(bf16[16,64,1024]{2,1,0:T(8,128)(2,1)} %convert_element_type.56), calls=%async_computation.3 | async-start | bytes 4194304 | tf_op jit(solution)/shard_map/all_to_all | solution.py:28
  160.8 142.4 %all-gather.5.cloned.1.call-start = ((), (), s32[]{:S(2)}) async-start(), calls=%async_computation.9 | async-start | bytes 11010048 | tf_op jit(solution)/shard_map/all_gather | solution.py:86
  209.9 53.4 %all-to-all-start.2 = ((bf16[16,256,256]{2,1,0:T(8,128)(2,1)}), bf16[16,256,256]{2,1,0:T(8,128)(2,1)}, u32[]{:S(2)}, u32[]{:S(2)}) async-start(bf16[16,256,256]{2,1,0:T(8,128)(2,1)} %get-tuple-element.16), calls=%async_computation.2 | async-start | bytes 4194304 | tf_op jit(solution)/shard_map/all_to_all | solution.py:25
  219.5 48.7 %copy-start.3 = (f32[64,1024]{1,0:T(8,128)S(1)}, f32[64,1024]{1,0:T(8,128)}, u32[]{:S(2)}) copy-start(f32[64,1024]{1,0:T(8,128)} %param.19) | copy-start | bytes 786436
  263.3 29.7 %all-to-all-start.4 = ((bf16[2,512,1024]{2,0,1:T(2,128)(2,1)}), bf16[2,512,1024]{2,0,1:T(2,128)(2,1)}, u32[]{:S(2)}, u32[]{:S(2)}) async-start(bf16[2,512,1024]{2,0,1:T(2,128)(2,1)} %copy.55), calls=%async_computation.4 | async-start | bytes 4194304 | tf_op jit(solution)/shard_map/all_to_all | solution.py:27
  268.1 54.1 %all-gather.11.cloned.1.call-start = ((), (), s32[]{:S(2)}) async-start(), calls=%async_computation.13 | async-start | bytes 1179648 | tf_op jit(solution)/shard_map/all_gather | solution.py:40
  268.9 151.0 %reduce-scatter.3.cloned.1.call-start = ((), (), s32[]{:S(2)}) async-start(), calls=%async_computation.10 | async-start | bytes 11010048 | tf_op jit(solution)/shard_map/reduce_scatter | solution.py:95
  322.2 102.1 %all-to-all-start.6 = ((bf16[2,256,1024]{2,1,0:T(8,128)(2,1)}), bf16[2,256,1024]{2,1,0:T(8,128)(2,1)}, u32[]{:S(2)}, u32[]{:S(2)}) async-start(bf16[2,256,1024]{2,1,0:T(8,128)(2,1)} %bitcast.93), calls=%async_computation.7 | async-start | bytes 2097152 | tf_op jit(solution)/shard_map/all_to_all | solution.py:42
  424.2 4.7 copy-start.4
  424.2 4.7 copy-start.7
  424.2 104.2 %all-to-all-start.5 = ((bf16[8,2,112,1024]{3,2,1,0:T(8,128)(2,1)}), bf16[8,2,112,1024]{3,2,1,0:T(8,128)(2,1)}, u32[]{:S(2)}, u32[]{:S(2)}) async-start(bf16[8,2,112,1024]{3,2,1,0:T(8,128)(2,1)} %copy.58), calls=%async_computation.6 | async-start | bytes 7340032 | tf_op jit(solution)/shard_map/all_to_all | solution.py:98
  428.9 35.3 %all-gather.7.cloned.1.call-start = ((), (), s32[]{:S(2)}) async-start(), calls=%async_computation.11 | async-start | bytes 1179648 | tf_op jit(solution)/shard_map/all_gather | solution.py:38
  430.7 84.7 %all-gather.9.cloned.1.call-start = ((), (), s32[]{:S(2)}) async-start(), calls=%async_computation.12 | async-start | bytes 1179648 | tf_op jit(solution)/shard_map/all_gather | solution.py:39
  431.3 112.9 %reduce-scatter.5.cloned.1.call-start = ((), (), s32[]{:S(2)}) async-start(), calls=%async_computation.14 | async-start | bytes 1376256 | tf_op jit(solution)/shard_map/reduce_scatter | solution.py:54
  515.4 3.7 copy-start.6
  541.0 5.4 copy-start
  544.2 3.1 copy-start.1
Sparse Core Ops, SparseCore 0:
  165.5 93.4 all-gather.4
  271.1 21.6 all-gather.10
  322.3 97.5 reduce-scatter.2
  431.6 32.5 all-gather.6
  466.2 49.1 all-gather.8
  519.2 17.4 reduce-scatter.4
where the time goes:
time: 556 us; the launch traced here: 555 us
  waiting for transfers between devices  377 us (68%)
  local copies, waits for them, and re-layouts  64.9 us (12%)
  starting transfers between devices  34.2 us (6%)
  matrix products  27.4 us (5%)
  other arithmetic  23.9 us (4%)
  between operations  14.4 us (3%)
  blocking collectives  13.6 us (2%)
    reduce_scatter x1, waiting for transfers between devices, per_device(): lax.psum_scatter(partial_rows.astype(jnp.bfloat16), 'tp', scatter_dimensi...  93.3 us
    all_to_all x1, waiting for transfers between devices, per_device(): lax.all_to_all(send_rows, 'fs', split_axis=0, concat_axis=0, tiled=True)  78.9 us
    all_gather x1, waiting for transfers between devices, per_device(): lax.all_gather(shared_up_cast, 'fs', axis=0, tiled=True)  47.4 us
    all_to_all x1, waiting for transfers between devices, per_device(): lax.all_to_all(down_cast, 'fs', split_axis=0, concat_axis=1, tiled=True)  44.5 us
    all_to_all x1, waiting for transfers between devices, per_device(): lax.all_to_all(up_cast, 'fs', split_axis=0, concat_axis=1, tiled=True)  43.8 us
    all_gather x1, waiting for transfers between devices, per_device(): lax.all_gather(shared_gate_cast, 'fs', axis=0, tiled=True)  32.6 us
    all_to_all x1, waiting for transfers between devices, per_device(): lax.all_to_all(lax.all_to_all(down_cast, 'fs', split_axis=0, concat_axis=...  19.4 us
    all_gather x1, blocking collectives, per_device(): gathered = lax.all_gather(tokens, 'tp', axis=1, tiled=True)  13.6 us
  transfers between devices with their start and end apart: 13, of which 9 were waited for; matrix products, arithmetic and copies ran while one was open for 19% of the time, Pallas kernels for 0%

commit v1 on v0

v1 whole, which is shorter than its diff:
```python
import functools

import jax
import jax.numpy as jnp
from jax import lax
from jax.experimental import pallas as pl
from jax.experimental.pallas import tpu as pltpu
from jax.sharding import PartitionSpec as P

MESH = pl.DeviceIdType.MESH


def weights_kernel(sizes, *refs):
    groups, n, tps = sizes
    count = 6
    srcs, outs = refs[:count], refs[count:2 * count]
    local_sem, send_sem, recv_sem, pass_send, pass_recv = refs[2 * count:]
    grp, fs, tp = lax.axis_index("grp"), lax.axis_index("fs"), lax.axis_index("tp")
    band = n // tps

    def at(g, f, t):
        return {"grp": g, "fs": f, "tp": t}

    barrier = pltpu.get_barrier_semaphore()
    for o in range(n):
        for x in range(tps):
            if o or x:
                pl.semaphore_signal(
                    barrier, inc=1, device_id=at(grp, lax.rem(fs + o, n), lax.rem(tp + x, tps)), device_id_type=MESH
                )
    for y in range(1, groups):
        pl.semaphore_signal(barrier, inc=1, device_id=at(lax.rem(grp + y, groups), fs, tp), device_id_type=MESH)
    pl.semaphore_wait(barrier, n * tps - 1 + groups - 1)

    def src_of(k, peer, share):
        held = outs[k].shape[0]
        first = peer * held if srcs[k].shape[0] > held else 0
        if k in (0, 1, 3, 4):
            part = srcs[k].shape[1] // groups
            return srcs[k].at[pl.ds(first, held), pl.ds(pl.multiple_of(share * part, part), part), :]
        part = srcs[k].shape[2] // groups
        return srcs[k].at[pl.ds(first, held), :, pl.ds(pl.multiple_of(share * part, part), part)]

    def dst_of(k, source, source_tp, share):
        if k in (0, 1, 3, 4):
            rows = srcs[k].shape[1]
            part = rows // groups
            return outs[k].at[:, pl.ds(pl.multiple_of(source * rows + share * part, part), part), :]
        rows, cols = srcs[k].shape[1:]
        part = cols // groups
        return outs[k].at[
            :,
            pl.ds(pl.multiple_of(lax.rem(source, band) * rows, rows), rows),
            pl.ds(pl.multiple_of(source_tp * cols + share * part, part), part),
        ]

    def over_fs(k, slot, src, dst, where):
        return pltpu.make_async_remote_copy(
            src_ref=src, dst_ref=dst, send_sem=send_sem.at[k, slot[0]], recv_sem=recv_sem.at[k, slot[1]],
            device_id=where, device_id_type=MESH,
        )

    def over_grp(k, slot, block, y):
        return pltpu.make_async_remote_copy(
            src_ref=block, dst_ref=block, send_sem=pass_send.at[k, slot, y - 1], recv_sem=pass_recv.at[k, slot, y - 1],
            device_id=at(lax.rem(grp + y, groups), fs, tp), device_id_type=MESH,
        )

    home = fs // band
    mine = lax.rem(fs, band) * tps + tp
    kept = home == tp

    def own(k, g):
        return pltpu.make_async_copy(src_of(k, fs, g), dst_of(k, fs, tp, g), local_sem.at[k, g])

    def row_send(k, o):
        peer = lax.rem(fs + o, n)
        return over_fs(k, (o, o), src_of(k, peer, grp), dst_of(k, fs, tp, grp), at(grp, peer, tp))

    def down_send(k, o):
        peer = lax.rem(fs + o, n)
        return over_fs(k, (o, mine), src_of(k, peer, grp), dst_of(k, fs, tp, grp), at(grp, peer, home))

    for k in (0, 1, 2, 3, 4, 5):
        for o in range(1, n):
            (down_send if k in (2, 5) else row_send)(k, o).start()
        if k in (2, 5):
            @pl.when(kept)
            def _():
                for g in range(groups):
                    own(k, g).start()

            @pl.when(jnp.logical_not(kept))
            def _():
                down_send(k, 0).start()
        else:
            for g in range(groups):
                own(k, g).start()

    def row_arrived(k, o):
        source = lax.rem(fs + n - o, n)
        block = dst_of(k, source, tp, grp)
        over_fs(k, (o, o), block, block, at(grp, source, tp)).wait_recv()
        return block

    def down_block(k, q, x, share):
        return dst_of(k, tp * band + q, x, share)

    def is_own(q, x):
        return jnp.logical_and(tp * band + q == fs, tp == x)

    def others(k):
        for q in range(band):
            for x in range(tps):
                yield q, x, q * tps + x

    for k in (0, 1, 2, 3, 4, 5):
        if k in (2, 5):
            for q, x, slot in others(k):
                @pl.when(jnp.logical_not(is_own(q, x)))
                def _():
                    block = down_block(k, q, x, grp)
                    over_fs(k, (0, slot), block, block, at(grp, tp * band + q, x)).wait_recv()
                    for y in range(1, groups):
                        over_grp(k, slot, block, y).start()
        else:
            for o in range(1, n):
                block = row_arrived(k, o)
                for y in range(1, groups):
                    over_grp(k, o, block, y).start()

    for k in (0, 1, 2, 3, 4, 5):
        if k in (2, 5):
            for q, x, slot in others(k):
                @pl.when(jnp.logical_not(is_own(q, x)))
                def _():
                    for y in range(1, groups):
                        over_grp(k, slot, down_block(k, q, x, grp), y).wait_send()
                        over_grp(k, slot, down_block(k, q, x, lax.rem(grp + groups - y, groups)), y).wait_recv()
            for o in range(1, n):
                down_send(k, o).wait_send()

            @pl.when(kept)
            def _():
                for g in range(groups):
                    own(k, g).wait()

            @pl.when(jnp.logical_not(kept))
            def _():
                down_send(k, 0).wait_send()
        else:
            for o in range(1, n):
                source = lax.rem(fs + n - o, n)
                for y in range(1, groups):
                    over_grp(k, o, dst_of(k, source, tp, grp), y).wait_send()
                    over_grp(k, o, dst_of(k, source, tp, lax.rem(grp + groups - y, groups)), y).wait_recv()
                row_send(k, o).wait_send()
            for g in range(groups):
                own(k, g).wait()


def move_weights(sizes, gate, up, down, shared_gate, shared_up, shared_down):
    groups, n, tps = sizes
    held = gate.shape[0] // n

    def rows(a, lead):
        return jax.ShapeDtypeStruct((lead, n * a.shape[1], a.shape[2]), jnp.bfloat16)

    def downs(a, lead):
        return jax.ShapeDtypeStruct((lead, n // tps * a.shape[1], tps * a.shape[2]), jnp.bfloat16)

    return pl.pallas_call(
        functools.partial(weights_kernel, sizes),
        out_shape=(
            rows(gate, held), rows(up, held), downs(down, held),
            rows(shared_gate, 1), rows(shared_up, 1), downs(shared_down, 1),
        ),
        in_specs=[pl.BlockSpec(memory_space=pltpu.VMEM)] * 6,
        out_specs=[pl.BlockSpec(memory_space=pl.ANY)] * 6,
        scratch_shapes=[
            pltpu.SemaphoreType.DMA((6, groups)),
            pltpu.SemaphoreType.DMA((6, n)),
            pltpu.SemaphoreType.DMA((6, n)),
            pltpu.SemaphoreType.DMA((6, n, groups - 1)),
            pltpu.SemaphoreType.DMA((6, n, groups - 1)),
        ],
        compiler_params=pltpu.CompilerParams(
            collective_id=0, has_side_effects=True, vmem_limit_bytes=16 * 1024 * 1024
        ),
        cost_estimate=pl.CostEstimate(flops=400_000_000, bytes_accessed=20_000_000, transcendentals=0),
    )(gate, up, down, shared_gate, shared_up, shared_down)


def per_device(
    sizes,
    tokens,
    routes,
    route_weights,
    norm_gain,
    gate_experts,
    up_experts,
    down_experts,
    shared_gate,
    shared_up,
    shared_down,
):
    bf16, f32 = jnp.bfloat16, jnp.float32
    groups, n, tps = sizes
    width = tokens.shape[1] * tps
    experts_all = gate_experts.shape[0]
    held = experts_all // n
    gain_rows = norm_gain[None, :, None]
    moved = move_weights(
        sizes,
        (gate_experts * gain_rows).astype(bf16),
        (up_experts * gain_rows).astype(bf16),
        down_experts.astype(bf16),
        (shared_gate[None] * gain_rows).astype(bf16),
        (shared_up[None] * gain_rows).astype(bf16),
        shared_down[None].astype(bf16),
    )
    gate_local, up_local, down_local, sg, su, sd = moved
    sg, su, sd = sg[0], su[0], sd[0]

    gathered = lax.all_gather(tokens, "tp", axis=1, tiled=True)
    widened = gathered.astype(f32)
    normed = (widened * lax.rsqrt(jnp.mean(widened * widened, axis=1, keepdims=True) + 1e-06)).astype(bf16)
    chosen = routes[:, :, None] == jnp.arange(experts_all, dtype=jnp.int32)[None, None, :]
    per_expert = jnp.sum(jnp.where(chosen, route_weights[:, :, None], 0.0), axis=1)
    high = lax.reduce_precision(per_expert, 8, 7)
    pad = -(2 * experts_all) % 128
    packed = jnp.concatenate(
        [normed, high.astype(bf16), (per_expert - high).astype(bf16), jnp.zeros((normed.shape[0], pad), bf16)], axis=1
    )
    everyone = lax.all_gather(packed, "fs", axis=0, tiled=True)
    rows = everyone[:, :width]
    first = lax.axis_index("fs") * held
    scale = lax.dynamic_slice_in_dim(everyone, width + first, held, 1).astype(f32) + lax.dynamic_slice_in_dim(
        everyone, width + experts_all + first, held, 1
    ).astype(f32)

    def hidden(x, g, u):
        return jax.nn.silu(jnp.dot(x, g, preferred_element_type=f32)) * jnp.dot(x, u, preferred_element_type=f32)

    active = jnp.concatenate(
        [(hidden(rows, gate_local[j], up_local[j]) * scale[:, j:j + 1]).astype(bf16) for j in range(held)], axis=1
    )
    partial = jnp.dot(active, down_local.reshape(-1, width), preferred_element_type=f32).astype(bf16)
    own_rows = lax.psum_scatter(partial, "fs", scatter_dimension=0, tiled=True)
    shared_part = jnp.dot(hidden(normed, sg, su).astype(bf16), sd, preferred_element_type=f32)
    both = (own_rows.astype(f32) + shared_part).astype(bf16)
    mixed = lax.psum_scatter(both, "tp", scatter_dimension=1, tiled=True)
    return mixed, gate_local, up_local, down_local, sg, su, sd


def solution(mesh):
    sizes = (mesh.shape["grp"], mesh.shape["fs"], mesh.shape["tp"])
    return jax.shard_map(
        functools.partial(per_device, sizes),
        mesh=mesh,
        in_specs=(
            P(("grp", "fs"), "tp"),
            P(("grp", "fs"), None),
            P(("grp", "fs"), None),
            P("fs"),
            P(None, "fs", "tp"),
            P(None, "fs", "tp"),
            P(None, "fs", "tp"),
            P("fs", "tp"),
            P("fs", "tp"),
            P("fs", "tp"),
        ),
        out_specs=(
            P(("grp", "fs"), "tp"),
            P(("grp", "fs"), None, "tp"),
            P(("grp", "fs"), None, "tp"),
            P(("grp", "fs"), "tp", None),
            P("grp", "tp"),
            P("grp", "tp"),
            P(("grp", "tp"), None),
        ),
        check_vma=False,
    )
```

time: 556 us -> 382 us (0.69)
  waiting for transfers between devices: 377 us -> 114 us
  Pallas kernels: 0 us -> 185 us
  local copies, waits for them, and re-layouts: 64.9 us -> 19.1 us
  starting transfers between devices: 34.2 us -> 0.12 us
  other arithmetic: 23.9 us -> 10.3 us
    all_to_all x7 -> x0, waiting for transfers between devices: 203 us -> none  [the longest x1 78.9 us: per_device(): lax.all_to_all(send_rows, 'fs', split_axis=0, concat_axis=0, tiled=True)]
    pallas_call x0 -> x1, Pallas kernels: none -> 185 us  [move_weights(): pl.pallas_call(functools.partial(weights_kernel, sizes), out_shape=(rows(...]
    all_gather x4 -> x1, waiting for transfers between devices: 80 us -> 0.01 us  [per_device(): everyone = lax.all_gather(packed, 'fs', axis=0, tiled=True)]
    all_to_all x7 -> x0, starting transfers between devices: 33.6 us -> none  [the longest x1 6.49 us: per_device(): lax.all_to_all(gate_cast, 'fs', split_axis=0, concat_axis=1, tiled=True)]
    all_to_all x10 -> x0, local copies, waits for them, and re-layouts: 28.3 us -> none  [the longest x4 11.7 us: per_device(): lax.all_to_all(lax.all_to_all(down_cast, 'fs', split_axis=0, concat_axis=...]
    reduce_scatter x2, waiting for transfers between devices: 93.3 us -> 114 us  [the longest x1 96.6 us: per_device(): own_rows = lax.psum_scatter(partial, 'fs', scatter_dimension=0, tiled=True)]
    gather x2 -> x0, local copies, waits for them, and re-layouts: 16.4 us -> none  [the longest x1 9.81 us: per_device(): returned.reshape(experts_all * capacity, quarter)[target]]
    unnamed x22 -> x44, local copies, waits for them, and re-layouts: 4.56 us -> 16.9 us
  transfers between devices with their start and end apart: 13 -> 3, of which waited for: 9 -> 2; matrix products, arithmetic and copies ran while one was open for 19% -> 3% of each run, Pallas kernels for 0% -> 48%
where the time goes in v1:
time: 382 us; the launch traced here: 381 us
  Pallas kernels  185 us (48%)
  waiting for transfers between devices  114 us (30%)
  matrix products  24.3 us (6%)
  local copies, waits for them, and re-layouts  19.1 us (5%)
  blocking collectives  14.4 us (4%)
  between operations  14.1 us (4%)
  other arithmetic  10.3 us (3%)
    pallas_call x1, Pallas kernels, move_weights(): pl.pallas_call(functools.partial(weights_kernel, sizes), out_shape=(rows(...  185 us
    reduce_scatter x1, waiting for transfers between devices, per_device(): own_rows = lax.psum_scatter(partial, 'fs', scatter_dimension=0, tiled=True)  96.6 us
    reduce_scatter x1, waiting for transfers between devices, per_device(): mixed = lax.psum_scatter(both, 'tp', scatter_dimension=1, tiled=True)  17.6 us
    unnamed x44, local copies, waits for them, and re-layouts  16.9 us
    all_gather x1, blocking collectives, per_device(): gathered = lax.all_gather(tokens, 'tp', axis=1, tiled=True)  14.4 us
    dot_general x3, matrix products, hidden(): jnp.dot(x, g, preferred_element_type=f32)  9.1 us
  transfers between devices with their start and end apart: 3, of which 2 were waited for; matrix products, arithmetic and copies ran while one was open for 3% of the time, Pallas kernels for 48%

profile of v1, /device:TPU:0, one launch (start us, length us, event | category | flops | bytes accessed | tf_op | source)
XLA Modules:
  0.0 381.3 jit_solution(615560079022436894)
XLA Ops:
  7.2 0.0 copy-start.14
  7.2 0.0 copy-start.15
  7.2 0.0 all-gather.2.cloned.1.call-start
  7.2 14.4 %all_gather.6 = bf16[224,2048]{1,0:T(8,128)(2,1)S(1)} all-gather(bf16[224,1024]{1,0:T(8,128)(2,1)} %param.10), channel_id=1, replica_groups=mesh['grp'=2,'fs'=8,'tp'=2] {'tp'}, dimensions={1}, use_global_device_ids=true | all-gather | bytes 1376256 | tf_op jit(solution)/shard_map/all_gather | solution.py:225
  21.6 0.3 fusion.27
  21.9 0.2 fusion.28
  22.1 0.0 copy-done.14
  22.2 0.0 copy-done.15
  22.2 0.0 copy-start.12
  22.2 0.1 copy.21
  22.3 0.1 copy.22
  22.5 1.1 concatenate.6
  23.6 0.0 all-gather.2.cloned.1.call-update
  23.6 0.0 reduce-scatter.3.cloned.1.call-start
  23.7 0.0 copy-start.13
  23.7 0.0 copy-start.16
  23.7 2.5 convert_element_type.66.refs_2_
  26.3 0.0 copy-done.12
  26.3 0.0 copy-done.13
  26.3 0.0 copy-done.16
  26.3 1.1 fusion.47
  27.5 4.5 %multiply_convert_fusion = (bf16[16,256,256]{2,1,0:T(8,128)(2,1)S(1)}, bf16[16,256,256]{2,1,0:T(8,128)(2,1)S(1)}) fusion(f32[16,256,256]{2,1,0:T(8,128)} %param.15, f32[256]{0:T(256)S(1)} %copy-done.16, f32[16,256,256]{2,1,0:T(8,128)} %param.14), kind=kLoop, calls=%fused_computation.9 | loop fusion | flops 4194304 | bytes 12583936 | tf_op jit(solution)/shard_map/convert_element_type | solution.py:216
  32.0 184.8 %shard_map.153 = (bf16[2,2048,256]{2,1,0:T(8,128)(2,1)S(1)}, bf16[2,2048,256]{2,1,0:T(8,128)(2,1)S(1)}, bf16[2,256,2048]{2,1,0:T(8,128)(2,1)S(1)}, bf16[1,2048,2...) custom-call(bf16[16,256,256]{2,1,0:T(8,128)(2,1)S(1)} %get-tuple-element.26.refs_0_, ...), custom_call_target="tpu_custom_call" | custom-call | flops 400000000 | bytes 20000000 | tf_op jit(solution)/shard_map/pallas_call | solution.py:172
  216.8 0.0 copy-start
  216.8 1.0 copy-done
  217.8 0.0 copy-start.2
  217.8 1.0 copy-done.2
  218.7 1.3 copy-done.4
  220.1 1.3 copy-done.7
  221.4 1.3 copy-done.10
  222.7 1.6 convert_add_fusion
  224.3 0.0 slice-start
  224.4 0.8 slice_reduce_fusion.1
  225.2 0.0 copy-done.11
  225.2 0.0 slice-start.1
  225.2 5.4 %fusion.2 = f32[1792,256]{0,1:T(8,128)S(1)} fusion(bf16[1792,2176]{1,0:T(8,128)(2,1)} %all-gather.2.cloned.1.call-done, bf16[2,2048,256]{2,1,0:T(8,128)(2,1)S(1)} %copy-done.11), kind=kOutput, calls=%fused_computation.3 | convolution fusion | flops 1879048192 | bytes 10223616 | tf_op jit(solution)/shard_map/dot_general | solution.py:243
  230.6 0.0 slice-done
  230.6 0.0 slice-done.1
  230.6 0.0 copy-start.8
  230.6 2.1 fusion.6
  232.8 0.0 copy-done.8
  232.8 2.8 fusion.20
  235.5 0.0 copy-start.5
  235.6 2.8 fusion.23
  238.3 0.0 copy-done.5
  238.3 6.1 %convolution_convert_fusion = bf16[1792,2048]{1,0:T(8,128)(2,1)} fusion(bf16[512,2048]{1,0:T(8,128)(2,1)S(1)} %bitcast.34, bf16[1792,256]{0,1:T(8,128)(2,1)S(1)} %fusion.20, bf16[1792,256]{0,1:T(8,128)(2,1)S(1)} %fusion.23), kind=kOutput, calls=%fused_computation | convolution fusion | flops 3765436416 | bytes 11272192 | tf_op jit(solution)/shard_map/dot_general | solution.py:248
  244.5 0.0 reduce-scatter.3.cloned.1.call-update
  244.5 0.0 copy-start.1
  244.5 0.0 reduce-scatter.5.cloned.1.call-start
  244.5 1.1 copy-done.3
  245.7 1.6 fusion.52
  247.3 96.6 %reduce-scatter.3.cloned.1.call-done = bf16[224,2048]{1,0:T(8,128)(2,1)} async-done(((bf16[1792,2048]{1,0:T(8,128)(2,1)}), bf16[224,2048]{1,0:T(8,128)(2,1)}) %reduce-scatter.3.cloned.1.call-update) | async-done | bytes 917520 | tf_op jit(solution)/shard_map/reduce_scatter | solution.py:249
  343.9 0.0 copy-done.1
  343.9 3.5 fusion.26
  347.4 0.0 reduce-scatter.5.cloned.1.call-update
  347.5 17.6 %reduce-scatter.5.cloned.1.call-done = bf16[224,1024]{1,0:T(8,128)(2,1)} async-done(((bf16[224,2048]{1,0:T(8,128)(2,1)}), bf16[224,1024]{1,0:T(8,128)(2,1)}) %reduce-scatter.5.cloned.1.call-update) | async-done | bytes 458768 | tf_op jit(solution)/shard_map/reduce_scatter | solution.py:252
  365.0 3.2 copy.29
  368.2 0.0 copy-done.9
  368.2 1.3 copy.30
  369.5 1.0 copy-done.6
  370.6 1.3 copy.31
  371.9 1.0 copy.32
  372.9 1.0 copy.33
  373.8 1.0 copy.34
  (14 shorter events, 0.1 us)
Async XLA Ops:
  7.2 15.0 %copy-start.14 = (f32[224,6]{0,1:T(8,128)S(1)}, f32[224,6]{0,1:T(8,128)}, u32[]{:S(2)}) copy-start(f32[224,6]{0,1:T(8,128)} %param.12) | copy-start | bytes 16132
  7.2 15.0 %copy-start.15 = (s32[224,6]{0,1:T(8,128)S(1)}, s32[224,6]{0,1:T(8,128)}, u32[]{:S(2)}) copy-start(s32[224,6]{0,1:T(8,128)} %param.11) | copy-start | bytes 16132
  7.2 215.5 %all-gather.2.cloned.1.call-start = ((), (), s32[]{:S(2)}) async-start(), calls=%async_computation.2 | async-start | bytes 8773632 | tf_op jit(solution)/shard_map/all_gather | solution.py:235
  22.2 4.1 %copy-start.12 = (bf16[224,2048]{1,0:T(8,128)(2,1)}, bf16[224,2048]{1,0:T(8,128)(2,1)S(1)}, u32[]{:S(2)}) copy-start(bf16[224,2048]{1,0:T(8,128)(2,1)S(1)} %fusion.28) | copy-start | bytes 2752516
  23.6 320.3 %reduce-scatter.3.cloned.1.call-start = ((), (), s32[]{:S(2)}) async-start(), calls=%async_computation.3 | async-start | bytes 8257536 | tf_op jit(solution)/shard_map/reduce_scatter | solution.py:249
  23.7 2.6 copy-start.13
  23.7 2.6 copy-start.16
  216.8 1.0 copy-start
  217.8 1.0 copy-start.2
  218.7 1.3 copy-start.4
  220.1 1.3 copy-start.7
  221.4 1.3 copy-start.10
  222.7 2.4 copy-start.11
  224.3 6.3 %slice-start = ((s8[7798784]{0:T(1024)(128)(4,1)}), s8[3604480]{0:T(1024)(128)(4,1)S(1)}, s32[]{:S(2)}) async-start(s8[7798784]{0:T(1024)(128)(4,1)} %bitcast.35), calls=%async_computation.5 | async-start | bytes 7208960
  225.2 5.4 %slice-start.1 = ((s8[7798784]{0:T(1024)(128)(4,1)}), s8[4194304]{0:T(1024)(128)(4,1)S(1)}, s32[]{:S(2)}) async-start(s8[7798784]{0:T(1024)(128)(4,1)} %bitcast.35), calls=%async_computation.6 | async-start | bytes 8388608
  230.6 2.1 copy-start.8
  235.5 2.8 copy-start.5
  244.4 1.2 copy-start.3
  244.5 99.4 %copy-start.1 = (bf16[1,2048,256]{2,1,0:T(8,128)(2,1)S(1)}, bf16[1,2048,256]{2,1,0:T(8,128)(2,1)}, u32[]{:S(2)}) copy-start(bf16[1,2048,256]{2,1,0:T(8,128)(2,1)} %copy-done) | copy-start | bytes 3145732
  244.5 120.5 %reduce-scatter.5.cloned.1.call-start = ((), (), s32[]{:S(2)}) async-start(), calls=%async_computation.4 | async-start | bytes 1376256 | tf_op jit(solution)/shard_map/reduce_scatter | solution.py:252
  365.0 3.2 copy-start.9
  368.2 2.3 copy-start.6
Sparse Core Ops, SparseCore 0:
  23.8 159.9 all-gather.1
  244.6 99.2 reduce-scatter.2
  347.6 17.3 reduce-scatter.4

commit v2 on v1

--- a/solution.py
+++ b/solution.py
@@ -189,6 +189,132 @@
         ),
         cost_estimate=pl.CostEstimate(flops=400_000_000, bytes_accessed=20_000_000, transcendentals=0),
     )(gate, up, down, shared_gate, shared_up, shared_down)
+
+
+def combine_kernel(sizes, part, shared, out, near, held, across, summed, far, local_sem, near_s, near_r, x_s, x_r, z_s, z_r):
+    _, n, tps = sizes
+    chips = n // 2
+    grp, fs, tp = lax.axis_index("grp"), lax.axis_index("fs"), lax.axis_index("tp")
+    chip, core = fs // 2, lax.rem(fs, 2)
+    rows, cols = out.shape
+    f32 = jnp.float32
+    step = 32
+
+    def sibling():
+        return {"grp": grp, "fs": chip * 2 + 1 - core, "tp": tp}
+
+    def x_peer(x):
+        return {"grp": grp, "fs": fs, "tp": lax.rem(tp + x, tps)}
+
+    def z_peer(o):
+        return {"grp": grp, "fs": lax.rem(chip + o, chips) * 2 + core, "tp": tp}
+
+    barrier = pltpu.get_barrier_semaphore()
+    peers = [sibling()] + [x_peer(x) for x in range(1, tps)] + [z_peer(o) for o in range(1, chips)]
+    for peer in peers:
+        pl.semaphore_signal(barrier, inc=1, device_id=peer, device_id_type=MESH)
+    pl.semaphore_wait(barrier, len(peers))
+
+    def near_copy(o):
+        return pltpu.make_async_remote_copy(
+            src_ref=part.at[lax.rem(chip + o, chips) * 2 + 1 - core], dst_ref=near.at[o],
+            send_sem=near_s.at[o], recv_sem=near_r.at[o], device_id=sibling(), device_id_type=MESH,
+        )
+
+    def keep_copy(o):
+        return pltpu.make_async_copy(part.at[lax.rem(chip + o, chips) * 2 + core], held.at[o], local_sem.at[o])
+
+    def x_copy(o, x):
+        there = pl.multiple_of(lax.rem(tp + x, tps) * cols, cols)
+        return pltpu.make_async_remote_copy(
+            src_ref=held.at[o, :, pl.ds(there, cols)], dst_ref=across.at[x - 1, o],
+            send_sem=x_s.at[x - 1, o], recv_sem=x_r.at[x - 1, o], device_id=x_peer(x), device_id_type=MESH,
+        )
+
+    def z_copy(o):
+        return pltpu.make_async_remote_copy(
+            src_ref=summed.at[o], dst_ref=far.at[o], send_sem=z_s.at[o], recv_sem=z_r.at[o],
+            device_id=z_peer(o), device_id_type=MESH,
+        )
+
+    order = list(range(1, chips)) + [0]
+    for o in order:
+        near_copy(o).start()
+        keep_copy(o).start()
+    for o in order:
+        near_copy(o).wait_recv()
+        keep_copy(o).wait()
+
+        @pl.loop(0, rows // step)
+        def _(i):
+            r = pl.ds(pl.multiple_of(i * step, step), step)
+            total = held[o, r, :].astype(f32) + near[o, r, :].astype(f32)
+            if o == 0:
+                total = total + shared[r, :]
+            held[o, r, :] = total.astype(jnp.bfloat16)
+
+        for x in range(1, tps):
+            x_copy(o, x).start()
+    here = pl.ds(pl.multiple_of(tp * cols, cols), cols)
+    for o in order:
+        for x in range(1, tps):
+            x_copy(o, x).wait_recv()
+
+        @pl.loop(0, rows // step)
+        def _(i):
+            r = pl.ds(pl.multiple_of(i * step, step), step)
+            total = held[o, r, here].astype(f32)
+            for x in range(1, tps):
+                total = total + across[x - 1, o, r, :].astype(f32)
+            summed[o, r, :] = total.astype(jnp.bfloat16)
+
+        if o:
+            z_copy(o).start()
+    for o in range(1, chips):
+        z_copy(o).wait_recv()
+
+    @pl.loop(0, rows // step)
+    def _(i):
+        r = pl.ds(pl.multiple_of(i * step, step), step)
+        total = summed[0, r, :].astype(f32)
+        for o in range(1, chips):
+            total = total + far[o, r, :].astype(f32)
+        out[r, :] = total.astype(jnp.bfloat16)
+
+    for o in order:
+        near_copy(o).wait_send()
+        for x in range(1, tps):
+            x_copy(o, x).wait_send()
+        if o:
+            z_copy(o).wait_send()
+
+
+def combine(sizes, partial, shared_part):
+    _, n, tps = sizes
+    chips = n // 2
+    rows, width = shared_part.shape
+    cols = width // tps
+    bf16 = jnp.bfloat16
+    dma = pltpu.SemaphoreType.DMA
+    return pl.pallas_call(
+        functools.partial(combine_kernel, sizes),
+        out_shape=jax.ShapeDtypeStruct((rows, cols), bf16),
+        in_specs=[pl.BlockSpec(memory_space=pl.ANY), pl.BlockSpec(memory_space=pltpu.VMEM)],
+        out_specs=pl.BlockSpec(memory_space=pltpu.VMEM),
+        scratch_shapes=[
+            pltpu.VMEM((chips, rows, width), bf16),
+            pltpu.VMEM((chips, rows, width), bf16),
+            pltpu.VMEM((tps - 1, chips, rows, cols), bf16),
+            pltpu.VMEM((chips, rows, cols), bf16),
+            pltpu.VMEM((chips, rows, cols), bf16),
+            dma((chips,)), dma((chips,)), dma((chips,)),
+            dma((tps - 1, chips)), dma((tps - 1, chips)), dma((chips,)), dma((chips,)),
+        ],
+        compiler_params=pltpu.CompilerParams(
+            collective_id=1, has_side_effects=True, vmem_limit_bytes=min(60, 8 + 16 * chips * rows * width // 2**20 // 2) * 2**20
+        ),
+        cost_estimate=pl.CostEstimate(flops=200_000_000, bytes_accessed=20_000_000, transcendentals=0),
+    )(partial.reshape(n, rows, width), shared_part)
 
 
 def per_device(
@@ -246,10 +372,8 @@
         [(hidden(rows, gate_local[j], up_local[j]) * scale[:, j:j + 1]).astype(bf16) for j in range(held)], axis=1
     )
     partial = jnp.dot(active, down_local.reshape(-1, width), preferred_element_type=f32).astype(bf16)
-    own_rows = lax.psum_scatter(partial, "fs", scatter_dimension=0, tiled=True)
     shared_part = jnp.dot(hidden(normed, sg, su).astype(bf16), sd, preferred_element_type=f32)
-    both = (own_rows.astype(f32) + shared_part).astype(bf16)
-    mixed = lax.psum_scatter(both, "tp", scatter_dimension=1, tiled=True)
+    mixed = combine(sizes, partial, shared_part)
     return mixed, gate_local, up_local, down_local, sg, su, sd
 
 

time: 382 us -> 342 us (0.90)
  waiting for transfers between devices: 114 us -> 0.04 us
  Pallas kernels: 185 us -> 263 us
    reduce_scatter x2 -> x0, waiting for transfers between devices: 114 us -> none  [the longest x1 96.6 us: per_device(): own_rows = lax.psum_scatter(partial, 'fs', scatter_dimension=0, tiled=True)]
    pallas_call x0 -> x1, Pallas kernels: none -> 78 us  [combine(): pl.pallas_call(functools.partial(combine_kernel, sizes), out_shape=jax.Sh...]
    unnamed x44 -> x41, local copies, waits for them, and re-layouts: 16.9 us -> 14.8 us
  transfers between devices with their start and end apart: 3 -> 1, of which waited for: 2 -> 0; matrix products, arithmetic and copies ran while one was open for 3% -> 4% of each run, Pallas kernels for 48% -> 54%
where the time goes in v2:
time: 342 us; the launch traced here: 341 us
  Pallas kernels  263 us (77%)
  matrix products  22.2 us (6%)
  local copies, waits for them, and re-layouts  17 us (5%)
  blocking collectives  14.4 us (4%)
  between operations  14.4 us (4%)
  other arithmetic  10.3 us (3%)
    pallas_call x1, Pallas kernels, move_weights(): pl.pallas_call(functools.partial(weights_kernel, sizes), out_shape=(rows(...  185 us
    pallas_call x1, Pallas kernels, combine(): pl.pallas_call(functools.partial(combine_kernel, sizes), out_shape=jax.Sh...  78 us
    unnamed x41, local copies, waits for them, and re-layouts  14.8 us
    all_gather x1, blocking collectives, per_device(): gathered = lax.all_gather(tokens, 'tp', axis=1, tiled=True)  14.4 us
    dot_general x3, matrix products, hidden(): jnp.dot(x, g, preferred_element_type=f32)  9.55 us
  transfers between devices with their start and end apart: 1, of which 0 were waited for; matrix products, arithmetic and copies ran while one was open for 4% of the time, Pallas kernels for 54%

profile of v2, /device:TPU:0, one launch (start us, length us, event | category | flops | bytes accessed | tf_op | source)
XLA Modules:
  0.0 341.3 jit_solution(1599868780212698877)
XLA Ops:
  7.2 0.0 copy-start.12
  7.2 0.0 copy-start.13
  7.2 0.0 all-gather.2.cloned.1.call-start
  7.2 14.4 %all_gather.6 = bf16[224,2048]{1,0:T(8,128)(2,1)S(1)} all-gather(bf16[224,1024]{1,0:T(8,128)(2,1)} %param.10), channel_id=1, replica_groups=mesh['grp'=2,'fs'=8,'tp'=2] {'tp'}, dimensions={1}, use_global_device_ids=true | all-gather | bytes 1376256 | tf_op jit(solution)/shard_map/all_gather | solution.py:351
  21.6 0.3 fusion.26
  21.9 0.2 fusion.27
  22.1 0.0 copy-done.12
  22.2 0.0 copy-done.13
  22.2 0.0 copy-start.10
  22.2 0.1 copy.21
  22.3 0.1 copy.22
  22.5 1.1 concatenate.6
  23.6 0.0 all-gather.2.cloned.1.call-update
  23.6 0.0 copy-start.11
  23.6 0.0 copy-start.14
  23.7 2.6 convert_element_type.60.refs_2_
  26.2 0.0 copy-done.10
  26.2 0.0 copy-done.11
  26.3 0.0 copy-done.14
  26.3 1.1 fusion.47
  27.4 4.5 %multiply_convert_fusion = (bf16[16,256,256]{2,1,0:T(8,128)(2,1)S(1)}, bf16[16,256,256]{2,1,0:T(8,128)(2,1)S(1)}) fusion(f32[16,256,256]{2,1,0:T(8,128)} %param.15, f32[256]{0:T(256)S(1)} %copy-done.14, f32[16,256,256]{2,1,0:T(8,128)} %param.14), kind=kLoop, calls=%fused_computation.9 | loop fusion | flops 4194304 | bytes 12583936 | tf_op jit(solution)/shard_map/convert_element_type | solution.py:342
  31.9 184.9 %shard_map.153 = (bf16[2,2048,256]{2,1,0:T(8,128)(2,1)S(1)}, bf16[2,2048,256]{2,1,0:T(8,128)(2,1)S(1)}, bf16[2,256,2048]{2,1,0:T(8,128)(2,1)S(1)}, bf16[1,2048,2...) custom-call(bf16[16,256,256]{2,1,0:T(8,128)(2,1)S(1)} %get-tuple-element.26.refs_0_, ...), custom_call_target="tpu_custom_call" | custom-call | flops 400000000 | bytes 20000000 | tf_op jit(solution)/shard_map/pallas_call | solution.py:172
  216.8 0.0 copy-start
  216.8 1.0 copy-done
  217.8 0.0 copy-start.2
  217.8 1.0 copy-done.2
  218.7 0.0 copy-start.4
  218.7 1.3 copy-done.4
  220.0 0.0 copy-start.6
  220.1 1.3 copy-done.6
  221.4 0.0 copy-start.8
  221.4 1.3 copy-done.8
  222.7 1.9 fusion.52
  224.6 2.7 fusion.32.shared
  227.3 0.0 all-gather.2.cloned.1.call-done
  227.3 0.0 copy-start.9
  227.3 1.6 convert_add_fusion
  228.9 0.0 slice-start
  228.9 0.8 slice_reduce_fusion.1
  229.8 0.0 copy-done.9
  229.8 0.0 slice-start.1
  229.8 5.5 %fusion.2 = f32[1792,256]{0,1:T(8,128)S(1)} fusion(bf16[1792,2176]{1,0:T(8,128)(2,1)} %all-gather.2.cloned.1.call-done, bf16[2,2048,256]{2,1,0:T(8,128)(2,1)S(1)} %copy-done.9), kind=kOutput, calls=%fused_computation.3 | convolution fusion | flops 1879048192 | bytes 10223616 | tf_op jit(solution)/shard_map/dot_general | solution.py:369
  235.3 0.0 slice-done
  235.3 0.0 slice-done.1
  235.4 0.0 copy-start.7
  235.4 2.1 fusion.6
  237.5 0.0 copy-done.7
  237.5 3.0 fusion.20
  240.5 0.0 copy-start.5
  240.5 2.8 fusion.23
  243.2 0.0 copy-done.5
  243.3 4.3 %convolution_convert_fusion = bf16[1792,2048]{1,0:T(8,128)(2,1)S(1)} fusion(bf16[512,2048]{1,0:T(8,128)(2,1)S(1)} %bitcast.36, bf16[1792,256]{0,1:T(8,128)(2,1)S(1)} %fusion.20, bf16[1792,256]{0,1:T(8,128)(2,1)S(1)} %fusion.23), kind=kOutput, calls=%fused_computation | convolution fusion | flops 3765436416 | bytes 11272192 | tf_op jit(solution)/shard_map/dot_general | solution.py:374
  247.6 78.0 %shard_map.154 = bf16[224,1024]{1,0:T(8,128)(2,1)S(1)} custom-call(bf16[8,224,2048]{2,1,0:T(8,128)(2,1)S(1)} %bitcast.29, f32[224,2048]{1,0:T(8,128)S(1)} %fusion.32.shared), custom_call_target="tpu_custom_call" | custom-call | flops 200000000 | bytes 20000000 | tf_op jit(solution)/shard_map/pallas_call | solution.py:299
  325.5 0.8 copy.30
  326.3 1.3 copy.31
  327.6 1.3 copy.32
  329.0 0.0 copy-start.3
  329.0 1.3 copy.33
  330.3 0.6 copy-done.3
  330.9 0.0 copy-start.1
  330.9 1.0 copy.34
  331.9 0.6 copy-done.1
  332.5 1.0 copy.35
  333.5 1.0 copy.36
  (6 shorter events, 0.1 us)
Async XLA Ops:
  7.2 15.0 %copy-start.12 = (f32[224,6]{0,1:T(8,128)S(1)}, f32[224,6]{0,1:T(8,128)}, u32[]{:S(2)}) copy-start(f32[224,6]{0,1:T(8,128)} %param.12) | copy-start | bytes 16132
  7.2 15.0 %copy-start.13 = (s32[224,6]{0,1:T(8,128)S(1)}, s32[224,6]{0,1:T(8,128)}, u32[]{:S(2)}) copy-start(s32[224,6]{0,1:T(8,128)} %param.11) | copy-start | bytes 16132
  7.2 220.1 %all-gather.2.cloned.1.call-start = ((), (), s32[]{:S(2)}) async-start(), calls=%async_computation | async-start | bytes 8773632 | tf_op jit(solution)/shard_map/all_gather | solution.py:361
  22.2 4.0 %copy-start.10 = (bf16[224,2048]{1,0:T(8,128)(2,1)}, bf16[224,2048]{1,0:T(8,128)(2,1)S(1)}, u32[]{:S(2)}) copy-start(bf16[224,2048]{1,0:T(8,128)(2,1)S(1)} %fusion.27) | copy-start | bytes 2752516
  23.6 2.6 copy-start.11
  23.6 2.6 copy-start.14
  216.8 1.0 copy-start
  217.8 1.0 copy-start.2
  218.7 1.3 copy-start.4
  220.0 1.3 copy-start.6
  221.4 1.3 copy-start.8
  227.3 2.5 copy-start.9
  228.9 6.4 %slice-start = ((s8[7798784]{0:T(1024)(128)(4,1)}), s8[4194304]{0:T(1024)(128)(4,1)S(1)}, s32[]{:S(2)}) async-start(s8[7798784]{0:T(1024)(128)(4,1)} %bitcast.37), calls=%async_computation.1 | async-start | bytes 8388608
  229.8 5.6 %slice-start.1 = ((s8[7798784]{0:T(1024)(128)(4,1)}), s8[3604480]{0:T(1024)(128)(4,1)S(1)}, s32[]{:S(2)}) async-start(s8[7798784]{0:T(1024)(128)(4,1)} %bitcast.37), calls=%async_computation.2 | async-start | bytes 7208960
  235.4 2.1 copy-start.7
  240.5 2.8 copy-start.5
  329.0 2.0 copy-start.3
  330.9 1.6 copy-start.1
Sparse Core Ops, SparseCore 0:
  23.7 159.9 all-gather.1
